TPU v7x, 32 devices: a whole 2x2x4 slice. The times are simulated.
32 devices in a mesh: sp: 8 (over z, core), tp: 4 (over y, x).
Axes of the slice: x: 2, y: 2, z: 4, core: 2. Of those that a mesh axis runs over, the one named last changes fastest.
Arguments:
- target: bfloat16 [1024, 2048], P(('sp', 'tp')), may hold values from -3 to 3
- source: bfloat16 [6144, 2048], P(('sp', 'tp')), may hold values from -6 to 6
- target_gain: float32 [2048], replicated, may hold values from 0.1 to 1.9
- source_gain: float32 [2048], replicated, may hold values from 0.1 to 1.9
- query_weight: bfloat16 [2048, 2048], P(None, 'tp'), may hold values from -0.125 to 0.125
- key_matrix: bfloat16 [2048, 256], replicated, may hold values from -0.125 to 0.125
- value_matrix: bfloat16 [2048, 256], replicated, may hold values from -0.125 to 0.125
- query_gain: float32 [16, 128], P('tp'), may hold values from 0.24 to 20
- key_gain: float32 [2, 128], replicated, may hold values from 1.2 to 4
- out_weight: bfloat16 [2048, 2048], P('tp'), may hold values from -0.125 to 0.125
Outputs:
- updated_target: bfloat16 [1024, 2048], P(('sp', 'tp'))
All inputs are finite; a program needn't handle non-finite values.
Results may differ from a plain program's by a relative error of at most 0.018.
The roundings to bfloat16 on the way count: a program that leaves them out, or rounds other values in their place, can miss the bound.
Values may be sent and summed in bfloat16 or wider, within the bound.
A program may use at most 64 MiB of HBM per device.

v0:
```python
import math

import jax
import jax.numpy as jnp
from jax import lax
from jax.sharding import PartitionSpec as P

KEY_VALUE_HEADS = 2
HEAD_SIZE = 128


EPSILON = 1e-06


def normed(values_in, gain):
    return (
        values_in
        * lax.rsqrt(jnp.mean(values_in * values_in, axis=-1, keepdims=True) + EPSILON)
        * gain
    )


def softmax_step(running, scores, seg_values, form):
    maxima, totals, weighted = running
    new_maxima = jnp.maximum(maxima, jnp.max(scores, axis=-1))
    fading = jnp.exp(maxima - new_maxima)
    weights = jnp.exp(scores - new_maxima[..., None])
    totals = totals * fading + jnp.sum(weights, axis=-1)
    weighted = weighted * fading[..., None] + jnp.einsum(
        form, weights.astype(jnp.bfloat16), seg_values, preferred_element_type=jnp.float32
    )
    return (new_maxima, totals, weighted)


def in_blocks(advance, running, segment, own_rows, limit):
    length = segment[0].shape[0]
    shards = length // own_rows
    widest = max(own_rows, limit)
    per_block = max(
        [
            number
            for number in range(1, shards + 1)
            if shards % number == 0 and own_rows * number <= widest
        ]
    )
    blocks = shards // per_block
    shaped = tuple(
        (member.reshape((blocks, own_rows * per_block) + member.shape[1:]) for member in segment)
    )

    def one_turn(carried, portion):
        return (advance(carried, portion), None)

    return lax.scan(one_turn, running, shaped)[0]


def body(
    target,
    source,
    target_gain,
    source_gain,
    query_weight,
    key_matrix,
    value_matrix,
    query_gain,
    key_gain,
    out_weight,
):
    local_heads = query_weight.shape[1] // HEAD_SIZE
    score_scale = 1.0 / math.sqrt(HEAD_SIZE)
    target_normed = normed(target.astype(jnp.float32), target_gain).astype(jnp.bfloat16)
    segment = lax.all_gather(target_normed, "tp", axis=0, tiled=True)
    raw_queries = jnp.dot(segment, query_weight, preferred_element_type=jnp.float32)
    shaped = raw_queries.reshape(segment.shape[0], local_heads, HEAD_SIZE)
    query_vectors = normed(shaped, query_gain).astype(jnp.bfloat16)
    block_rows = query_vectors.shape[0]
    normed_source_rows = normed(source.astype(jnp.float32), source_gain).astype(jnp.bfloat16)
    unnormed_keys = jnp.dot(
        normed_source_rows, key_matrix, preferred_element_type=jnp.float32
    ).reshape(source.shape[0], KEY_VALUE_HEADS, HEAD_SIZE)
    key_rows = normed(unnormed_keys, key_gain).astype(jnp.bfloat16)
    value_vectors = (
        jnp.dot(normed_source_rows, value_matrix, preferred_element_type=jnp.float32)
        .astype(jnp.bfloat16)
        .reshape(source.shape[0], KEY_VALUE_HEADS, HEAD_SIZE)
    )
    each_head_view = lax.axis_size("tp") // KEY_VALUE_HEADS
    sent_keys = jnp.repeat(key_rows, each_head_view, axis=1)
    sent_values = jnp.repeat(value_vectors, each_head_view, axis=1)
    head_keys, head_values = (
        lax.all_to_all(sent_keys, "tp", split_axis=1, concat_axis=0, tiled=True),
        lax.all_to_all(sent_values, "tp", split_axis=1, concat_axis=0, tiled=True),
    )
    head_keys = head_keys.reshape(-1, HEAD_SIZE)
    head_values = head_values.reshape(-1, HEAD_SIZE)
    own_rows = head_keys.shape[0]
    small_shape = (block_rows, local_heads)
    initial = (
        jnp.full(small_shape, -1e30, jnp.float32),
        jnp.zeros(small_shape, jnp.float32),
        jnp.zeros(small_shape + (HEAD_SIZE,), jnp.float32),
    )

    def advance(carried, portion):
        scores = (
            jnp.einsum("rhd,nd->rhn", query_vectors, portion[0], preferred_element_type=jnp.float32)
            * score_scale
        )
        return softmax_step(carried, scores, portion[1], "rhn,nd->rhd")

    maxima, totals, weighted = in_blocks(
        advance,
        initial,
        (
            lax.all_gather(head_keys, "sp", axis=0, tiled=True),
            lax.all_gather(head_values, "sp", axis=0, tiled=True),
        ),
        own_rows,
        1024,
    )
    attended = (
        (weighted / totals[..., None])
        .astype(jnp.bfloat16)
        .reshape(block_rows, local_heads * HEAD_SIZE)
    )
    portion = attended
    update = lax.psum_scatter(
        jnp.dot(portion, out_weight, preferred_element_type=jnp.float32).astype(jnp.bfloat16),
        "tp",
        scatter_dimension=0,
        tiled=True,
    ).astype(jnp.float32)
    return (target.astype(jnp.float32) + update).astype(jnp.bfloat16)


def solution(mesh):
    return jax.shard_map(
        body,
        mesh=mesh,
        in_specs=(
            P(("sp", "tp"), None),
            P(("sp", "tp"), None),
            P(),
            P(),
            P(None, "tp"),
            P(),
            P(),
            P("tp", None),
            P(),
            P("tp", None),
        ),
        out_specs=P(("sp", "tp"), None),
        check_vma=False,
    )
```

profile of v0, /device:TPU:0, one launch (start us, length us, event | category | flops | bytes accessed | tf_op | source)
XLA Modules:
  0.0 152.2 jit_solution(7912109217960230163)
XLA Ops:
  6.5 1.5 fusion.12
  8.1 1.9 %fusion.23 = f32[192,256]{1,0:T(8,128)S(1)} fusion(bf16[2048,256]{1,0:T(8,128)(2,1)} %param.17, bf16[192,2048]{1,0:T(8,128)(2,1)} %param.13, f32[2048]{0:T(1024)} %param.15, f32[192]{0:T(256)S(1)} %add_rsqrt_fusion.2), kind=kOutput, calls=%fused_computation.39 | convolution fusion | flops 202899456 | bytes 2040576 | tf_op jit(solution)/shard_map/dot_general | solution.py:78
  10.0 0.0 copy-start.7
  10.0 0.1 reshape.71
  10.1 0.3 multiply_reduce_fusion.1
  10.5 0.3 multiply_convert_fusion
  10.8 10.6 %all_to_all.30 = bf16[192,4,128]{2,0,1:T(8,128)(2,1)} all-to-all(bf16[192,4,128]{2,0,1:T(8,128)(2,1)S(1)} %bitcast.70), channel_id=1, replica_groups=mesh['sp'=8,'tp'=4] {'tp'}, dimensions={1} | all-to-all | bytes 393216 | tf_op jit(solution)/shard_map/all_to_all | solution.py:91
  21.4 0.0 all-gather.3.cloned.1.call-update
  21.5 0.0 copy-start.2
  21.5 0.0 copy-start.4
  21.5 0.0 all-gather.5.cloned.1.call-start
  21.6 1.7 %fusion.15 = bf16[24,2,8,128]{3,2,1,0:T(8,128)(2,1)S(1)} fusion(bf16[2048,256]{1,0:T(8,128)(2,1)} %param.18, bf16[192,2048]{1,0:T(8,128)(2,1)S(1)} %copy-done.3, f32[2048]{0:T(1024)S(1)} %copy-done.7, f32[192]{0:T(256)S(1)} %add_rsqrt_fusion.2), kind=kOutput, calls=%fused_computation.26 | convolution fusion | flops 202948608 | bytes 1942272 | tf_op jit(solution)/shard_map/dot_general | solution.py:83
  23.3 8.6 %all_to_all.31 = bf16[192,4,128]{2,0,1:T(8,128)(2,1)} all-to-all(bf16[192,4,128]{2,0,1:T(8,128)(2,1)S(1)} %bitcast.71), channel_id=1, replica_groups=mesh['sp'=8,'tp'=4] {'tp'}, dimensions={1} | all-to-all | bytes 393216 | tf_op jit(solution)/shard_map/all_to_all | solution.py:92
  31.9 0.0 all-gather.5.cloned.1.call-update
  31.9 0.0 reduce-scatter.2.cloned.1.call-start
  32.0 0.1 fusion.16
  32.1 0.1 fusion.18
  32.2 10.0 %all_gather.10 = bf16[128,2048]{1,0:T(8,128)(2,1)S(1)} all-gather(bf16[32,2048]{1,0:T(8,128)(2,1)S(1)} %fusion.18), channel_id=1, replica_groups=mesh['sp'=8,'tp'=4] {'tp'}, dimensions={0}, use_global_device_ids=true | all-gather | bytes 655360 | tf_op jit(solution)/shard_map/all_gather | solution.py:72
  42.2 2.1 %fusion.25 = f32[128,512]{1,0:T(8,128)S(1)} fusion(bf16[128,2048]{1,0:T(8,128)(2,1)S(1)} %all_gather.10, bf16[2048,512]{1,0:T(8,128)(2,1)} %param.16), kind=kOutput, calls=%fused_computation.47 | convolution fusion | flops 268435456 | bytes 2883584 | tf_op jit(solution)/shard_map/dot_general | solution.py:73
  44.3 0.1 reshape.75
  44.4 0.2 multiply_reduce_fusion
  44.6 0.1 copy.37
  44.7 0.0 copy-done.5
  44.7 0.1 fusion.21
  44.8 1.6 %all-gather.3.cloned.1.call-done = bf16[6144,128]{1,0:T(8,128)(2,1)} async-done(((bf16[768,128]{1,0:T(8,128)(2,1)}), bf16[6144,128]{1,0:T(8,128)(2,1)}) %all-gather.3.cloned.1.call-update) | async-done | bytes 1572880 | tf_op jit(solution)/shard_map/all_gather | solution.py:115
  46.4 26.1 %all-gather.5.cloned.1.call-done = bf16[6144,128]{1,0:T(8,128)(2,1)} async-done(((bf16[768,128]{1,0:T(8,128)(2,1)}), bf16[6144,128]{1,0:T(8,128)(2,1)}) %all-gather.5.cloned.1.call-update) | async-done | bytes 1572880 | tf_op jit(solution)/shard_map/all_gather | solution.py:116
  72.5 45.7 %while.15 = (s32[]{:T(128)}, f32[128,4]{0,1:T(4,128)S(1)}, f32[128,4]{0,1:T(4,128)S(1)}, f32[128,4,128]{2,0,1:T(8,128)S(1)}, bf16[8,768,128]{2,1,0:T(8,128)(2,1)...) while((s32[]{:T(128)}, f32[128,4]{0,1:T(4,128)S(1)}, ...), condition=%wide.region_7.8_spmd.clone, body=%wide.region_4.7_spmd.clone.sunk | while | flops 203885056 | bytes 12092549 | solution.py:54
  72.5 2.4 %bitcast_reduce_fusion.2 = (f32[128,4]{0,1:T(4,128)S(1)}, f32[768,128,4]{1,0,2:T(8,128)}) fusion(bf16[128,4,128]{2,0,1:T(8,128)(2,1)S(1)} %get-tuple-element.161, bf16[8,768,128]{2,1,0:T(8,128)(2,1)} %get-tuple-element.160, s32[]{:T(128)} %get-tuple-element.147), kind=kOutput, calls=%fused_computation.1.clone.1 | convolution fusion | flops 101449216 | bytes 1903104 | tf_op jit(solution)/shard_map/while/body/eval_jaxpr/rhd,nd->rhn/dot_general | solution.py:106
  75.0 1.8 %fusion.42 = f32[128,4]{0,1:T(4,128)S(1)} fusion(f32[768,128,4]{1,0,2:T(8,128)} %get-tuple-element.135, f32[128,4]{0,1:T(4,128)S(1)} %select_maximum_fusion.2), kind=kLoop, calls=%fused_computation.5.clone.1 | loop fusion | flops 785920 | bytes 1576960 | tf_op jit(solution)/shard_map/while/body/eval_jaxpr/reduce_sum | solution.py:28
  76.7 0.1 copy-done.1
  76.8 1.4 convolution_add_fusion.2
  78.2 2.4 %bitcast_reduce_fusion.2 = (f32[128,4]{0,1:T(4,128)S(1)}, f32[768,128,4]{1,0,2:T(8,128)}) fusion(bf16[128,4,128]{2,0,1:T(8,128)(2,1)S(1)} %get-tuple-element.161, bf16[8,768,128]{2,1,0:T(8,128)(2,1)} %get-tuple-element.160, s32[]{:T(128)} %get-tuple-element.147), kind=kOutput, calls=%fused_computation.1.clone.1 | convolution fusion | flops 101449216 | bytes 1903104 | tf_op jit(solution)/shard_map/while/body/eval_jaxpr/rhd,nd->rhn/dot_general | solution.py:106
  80.7 1.8 %fusion.42 = f32[128,4]{0,1:T(4,128)S(1)} fusion(f32[768,128,4]{1,0,2:T(8,128)} %get-tuple-element.135, f32[128,4]{0,1:T(4,128)S(1)} %select_maximum_fusion.2), kind=kLoop, calls=%fused_computation.5.clone.1 | loop fusion | flops 785920 | bytes 1576960 | tf_op jit(solution)/shard_map/while/body/eval_jaxpr/reduce_sum | solution.py:28
  82.4 0.1 copy-done.1
  82.5 1.4 convolution_add_fusion.2
  83.9 2.4 %bitcast_reduce_fusion.2 = (f32[128,4]{0,1:T(4,128)S(1)}, f32[768,128,4]{1,0,2:T(8,128)}) fusion(bf16[128,4,128]{2,0,1:T(8,128)(2,1)S(1)} %get-tuple-element.161, bf16[8,768,128]{2,1,0:T(8,128)(2,1)} %get-tuple-element.160, s32[]{:T(128)} %get-tuple-element.147), kind=kOutput, calls=%fused_computation.1.clone.1 | convolution fusion | flops 101449216 | bytes 1903104 | tf_op jit(solution)/shard_map/while/body/eval_jaxpr/rhd,nd->rhn/dot_general | solution.py:106
  86.4 1.8 %fusion.42 = f32[128,4]{0,1:T(4,128)S(1)} fusion(f32[768,128,4]{1,0,2:T(8,128)} %get-tuple-element.135, f32[128,4]{0,1:T(4,128)S(1)} %select_maximum_fusion.2), kind=kLoop, calls=%fused_computation.5.clone.1 | loop fusion | flops 785920 | bytes 1576960 | tf_op jit(solution)/shard_map/while/body/eval_jaxpr/reduce_sum | solution.py:28
  88.1 0.1 copy-done.1
  88.3 1.4 convolution_add_fusion.2
  89.6 2.4 %bitcast_reduce_fusion.2 = (f32[128,4]{0,1:T(4,128)S(1)}, f32[768,128,4]{1,0,2:T(8,128)}) fusion(bf16[128,4,128]{2,0,1:T(8,128)(2,1)S(1)} %get-tuple-element.161, bf16[8,768,128]{2,1,0:T(8,128)(2,1)} %get-tuple-element.160, s32[]{:T(128)} %get-tuple-element.147), kind=kOutput, calls=%fused_computation.1.clone.1 | convolution fusion | flops 101449216 | bytes 1903104 | tf_op jit(solution)/shard_map/while/body/eval_jaxpr/rhd,nd->rhn/dot_general | solution.py:106
  92.1 1.8 %fusion.42 = f32[128,4]{0,1:T(4,128)S(1)} fusion(f32[768,128,4]{1,0,2:T(8,128)} %get-tuple-element.135, f32[128,4]{0,1:T(4,128)S(1)} %select_maximum_fusion.2), kind=kLoop, calls=%fused_computation.5.clone.1 | loop fusion | flops 785920 | bytes 1576960 | tf_op jit(solution)/shard_map/while/body/eval_jaxpr/reduce_sum | solution.py:28
  93.9 0.1 copy-done.1
  94.0 1.4 convolution_add_fusion.2
  95.4 2.4 %bitcast_reduce_fusion.2 = (f32[128,4]{0,1:T(4,128)S(1)}, f32[768,128,4]{1,0,2:T(8,128)}) fusion(bf16[128,4,128]{2,0,1:T(8,128)(2,1)S(1)} %get-tuple-element.161, bf16[8,768,128]{2,1,0:T(8,128)(2,1)} %get-tuple-element.160, s32[]{:T(128)} %get-tuple-element.147), kind=kOutput, calls=%fused_computation.1.clone.1 | convolution fusion | flops 101449216 | bytes 1903104 | tf_op jit(solution)/shard_map/while/body/eval_jaxpr/rhd,nd->rhn/dot_general | solution.py:106
  97.8 1.8 %fusion.42 = f32[128,4]{0,1:T(4,128)S(1)} fusion(f32[768,128,4]{1,0,2:T(8,128)} %get-tuple-element.135, f32[128,4]{0,1:T(4,128)S(1)} %select_maximum_fusion.2), kind=kLoop, calls=%fused_computation.5.clone.1 | loop fusion | flops 785920 | bytes 1576960 | tf_op jit(solution)/shard_map/while/body/eval_jaxpr/reduce_sum | solution.py:28
  99.6 0.1 copy-done.1
  99.7 1.4 convolution_add_fusion.2
  101.1 2.4 %bitcast_reduce_fusion.2 = (f32[128,4]{0,1:T(4,128)S(1)}, f32[768,128,4]{1,0,2:T(8,128)}) fusion(bf16[128,4,128]{2,0,1:T(8,128)(2,1)S(1)} %get-tuple-element.161, bf16[8,768,128]{2,1,0:T(8,128)(2,1)} %get-tuple-element.160, s32[]{:T(128)} %get-tuple-element.147), kind=kOutput, calls=%fused_computation.1.clone.1 | convolution fusion | flops 101449216 | bytes 1903104 | tf_op jit(solution)/shard_map/while/body/eval_jaxpr/rhd,nd->rhn/dot_general | solution.py:106
  103.5 1.8 %fusion.42 = f32[128,4]{0,1:T(4,128)S(1)} fusion(f32[768,128,4]{1,0,2:T(8,128)} %get-tuple-element.135, f32[128,4]{0,1:T(4,128)S(1)} %select_maximum_fusion.2), kind=kLoop, calls=%fused_computation.5.clone.1 | loop fusion | flops 785920 | bytes 1576960 | tf_op jit(solution)/shard_map/while/body/eval_jaxpr/reduce_sum | solution.py:28
  105.3 0.1 copy-done.1
  105.4 1.4 convolution_add_fusion.2
  106.8 2.4 %bitcast_reduce_fusion.2 = (f32[128,4]{0,1:T(4,128)S(1)}, f32[768,128,4]{1,0,2:T(8,128)}) fusion(bf16[128,4,128]{2,0,1:T(8,128)(2,1)S(1)} %get-tuple-element.161, bf16[8,768,128]{2,1,0:T(8,128)(2,1)} %get-tuple-element.160, s32[]{:T(128)} %get-tuple-element.147), kind=kOutput, calls=%fused_computation.1.clone.1 | convolution fusion | flops 101449216 | bytes 1903104 | tf_op jit(solution)/shard_map/while/body/eval_jaxpr/rhd,nd->rhn/dot_general | solution.py:106
  109.2 1.8 %fusion.42 = f32[128,4]{0,1:T(4,128)S(1)} fusion(f32[768,128,4]{1,0,2:T(8,128)} %get-tuple-element.135, f32[128,4]{0,1:T(4,128)S(1)} %select_maximum_fusion.2), kind=kLoop, calls=%fused_computation.5.clone.1 | loop fusion | flops 785920 | bytes 1576960 | tf_op jit(solution)/shard_map/while/body/eval_jaxpr/reduce_sum | solution.py:28
  111.0 0.1 copy-done.1
  111.1 1.4 convolution_add_fusion.2
  112.5 2.4 %bitcast_reduce_fusion.2 = (f32[128,4]{0,1:T(4,128)S(1)}, f32[768,128,4]{1,0,2:T(8,128)}) fusion(bf16[128,4,128]{2,0,1:T(8,128)(2,1)S(1)} %get-tuple-element.161, bf16[8,768,128]{2,1,0:T(8,128)(2,1)} %get-tuple-element.160, s32[]{:T(128)} %get-tuple-element.147), kind=kOutput, calls=%fused_computation.1.clone.1 | convolution fusion | flops 101449216 | bytes 1903104 | tf_op jit(solution)/shard_map/while/body/eval_jaxpr/rhd,nd->rhn/dot_general | solution.py:106
  114.9 1.8 %fusion.42 = f32[128,4]{0,1:T(4,128)S(1)} fusion(f32[768,128,4]{1,0,2:T(8,128)} %get-tuple-element.135, f32[128,4]{0,1:T(4,128)S(1)} %select_maximum_fusion.2), kind=kLoop, calls=%fused_computation.5.clone.1 | loop fusion | flops 785920 | bytes 1576960 | tf_op jit(solution)/shard_map/while/body/eval_jaxpr/reduce_sum | solution.py:28
  116.7 0.1 copy-done.1
  116.8 1.4 convolution_add_fusion.2
  118.2 0.1 copy.40
  118.4 1.3 convolution_convert_fusion
  119.6 0.0 reduce-scatter.2.cloned.1.call-update
  119.7 24.4 %reduce-scatter.2.cloned.1.call-done = bf16[32,2048]{1,0:T(8,128)(2,1)} async-done(((bf16[128,2048]{1,0:T(8,128)(2,1)}), bf16[32,2048]{1,0:T(8,128)(2,1)}) %reduce-scatter.2.cloned.1.call-update) | async-done | bytes 131088 | tf_op jit(solution)/shard_map/reduce_scatter | solution.py:127
  144.1 1.6 %fusion.19 = bf16[32,2048]{1,0:T(8,128)(2,1)} fusion(bf16[32,2048]{1,0:T(8,128)(2,1)S(1)} %copy-done.2, bf16[32,2048]{1,0:T(8,128)(2,1)} %reduce-scatter.2.cloned.1.call-done), kind=kLoop, calls=%fused_computation.33 | loop fusion | flops 262144 | bytes 393216 | tf_op jit(solution)/shard_map/convert_element_type | solution.py:133
  (55 shorter events, 0.4 us)
Async XLA Ops:
  6.5 111.8 %copy-start = (bf16[512,2048]{1,0:T(8,128)(2,1)S(1)}, bf16[512,2048]{1,0:T(8,128)(2,1)}, u32[]{:S(2)}) copy-start(bf16[512,2048]{1,0:T(8,128)(2,1)} %param.21) | copy-start | bytes 6291460
  6.5 39.9 %all-gather.3.cloned.1.call-start = ((), (), s32[]{:S(2)}) async-start(), calls=%async_computation.3 | async-start | bytes 1769472 | tf_op jit(solution)/shard_map/all_gather | solution.py:115
  8.1 2.4 %copy-start.6 = (f32[2,128]{1,0:T(2,128)S(1)}, f32[2,128]{1,0:T(2,128)}, u32[]{:S(2)}) copy-start(f32[2,128]{1,0:T(2,128)} %param.20) | copy-start | bytes 3076
  10.0 11.5 %copy-start.3 = (bf16[192,2048]{1,0:T(8,128)(2,1)S(1)}, bf16[192,2048]{1,0:T(8,128)(2,1)}, u32[]{:S(2)}) copy-start(bf16[192,2048]{1,0:T(8,128)(2,1)} %param.13) | copy-start | bytes 2359300
  10.0 11.5 %copy-start.7 = (f32[2048]{0:T(1024)S(1)}, f32[2048]{0:T(1024)}, u32[]{:S(2)}) copy-start(f32[2048]{0:T(1024)} %param.15) | copy-start | bytes 24580
  21.5 10.5 %copy-start.2 = (bf16[32,2048]{1,0:T(8,128)(2,1)S(1)}, bf16[32,2048]{1,0:T(8,128)(2,1)}, u32[]{:S(2)}) copy-start(bf16[32,2048]{1,0:T(8,128)(2,1)} %param.12) | copy-start | bytes 393220
  21.5 10.7 %copy-start.4 = (f32[2048]{0:T(1024)S(1)}, f32[2048]{0:T(1024)}, u32[]{:S(2)}) copy-start(f32[2048]{0:T(1024)} %param.14) | copy-start | bytes 24580
  21.5 51.0 %all-gather.5.cloned.1.call-start = ((), (), s32[]{:S(2)}) async-start(), calls=%async_computation.4 | async-start | bytes 1769472 | tf_op jit(solution)/shard_map/all_gather | solution.py:116
  31.9 112.2 %reduce-scatter.2.cloned.1.call-start = ((), (), s32[]{:S(2)}) async-start(), calls=%async_computation.5 | async-start | bytes 655360 | tf_op jit(solution)/shard_map/reduce_scatter | solution.py:127
  42.2 2.5 %copy-start.5 = (f32[4,128]{1,0:T(4,128)S(1)}, f32[4,128]{1,0:T(4,128)}, u32[]{:S(2)}) copy-start(f32[4,128]{1,0:T(4,128)} %param.19) | copy-start | bytes 6148
  75.0 1.9 %copy-start.1 = (f32[768,128,4]{1,0,2:T(8,128)S(1)}, f32[768,128,4]{1,0,2:T(8,128)}, u32[]{:S(2)}) copy-start(f32[768,128,4]{1,0,2:T(8,128)} %get-tuple-element.135) | copy-start | bytes 4718596 | tf_op jit(solution)/shard_map/while
  80.7 1.9 %copy-start.1 = (f32[768,128,4]{1,0,2:T(8,128)S(1)}, f32[768,128,4]{1,0,2:T(8,128)}, u32[]{:S(2)}) copy-start(f32[768,128,4]{1,0,2:T(8,128)} %get-tuple-element.135) | copy-start | bytes 4718596 | tf_op jit(solution)/shard_map/while
  86.4 1.9 %copy-start.1 = (f32[768,128,4]{1,0,2:T(8,128)S(1)}, f32[768,128,4]{1,0,2:T(8,128)}, u32[]{:S(2)}) copy-start(f32[768,128,4]{1,0,2:T(8,128)} %get-tuple-element.135) | copy-start | bytes 4718596 | tf_op jit(solution)/shard_map/while
  92.1 1.9 %copy-start.1 = (f32[768,128,4]{1,0,2:T(8,128)S(1)}, f32[768,128,4]{1,0,2:T(8,128)}, u32[]{:S(2)}) copy-start(f32[768,128,4]{1,0,2:T(8,128)} %get-tuple-element.135) | copy-start | bytes 4718596 | tf_op jit(solution)/shard_map/while
  97.8 1.9 %copy-start.1 = (f32[768,128,4]{1,0,2:T(8,128)S(1)}, f32[768,128,4]{1,0,2:T(8,128)}, u32[]{:S(2)}) copy-start(f32[768,128,4]{1,0,2:T(8,128)} %get-tuple-element.135) | copy-start | bytes 4718596 | tf_op jit(solution)/shard_map/while
  103.5 1.9 %copy-start.1 = (f32[768,128,4]{1,0,2:T(8,128)S(1)}, f32[768,128,4]{1,0,2:T(8,128)}, u32[]{:S(2)}) copy-start(f32[768,128,4]{1,0,2:T(8,128)} %get-tuple-element.135) | copy-start | bytes 4718596 | tf_op jit(solution)/shard_map/while
  109.2 1.9 %copy-start.1 = (f32[768,128,4]{1,0,2:T(8,128)S(1)}, f32[768,128,4]{1,0,2:T(8,128)}, u32[]{:S(2)}) copy-start(f32[768,128,4]{1,0,2:T(8,128)} %get-tuple-element.135) | copy-start | bytes 4718596 | tf_op jit(solution)/shard_map/while
  114.9 1.9 %copy-start.1 = (f32[768,128,4]{1,0,2:T(8,128)S(1)}, f32[768,128,4]{1,0,2:T(8,128)}, u32[]{:S(2)}) copy-start(f32[768,128,4]{1,0,2:T(8,128)} %get-tuple-element.135) | copy-start | bytes 4718596 | tf_op jit(solution)/shard_map/while
Sparse Core Ops, SparseCore 0:
  21.6 24.7 all-gather.2
  48.1 24.4 all-gather.4
  119.8 24.2 reduce-scatter.1
where the time goes:
time: 153 us; the launch traced here: 152 us
  waiting for transfers between devices  52.1 us (34%)
  matrix products  37.3 us (24%)
  blocking collectives  29.2 us (19%)
  other arithmetic  18.5 us (12%)
  between operations  13.4 us (9%)
    all_gather x1, waiting for transfers between devices, body(): lax.all_gather(head_values, 'sp', axis=0, tiled=True)  26.1 us
    reduce_scatter x1, waiting for transfers between devices, body(): lax.psum_scatter(jnp.dot(portion, out_weight, preferred_element_type=jnp....  24.4 us
    dot_general x8, matrix products, advance(): jnp.einsum('rhd,nd->rhn', query_vectors, portion[0], preferred_element_ty...  19.4 us
    reduce_sum x8, other arithmetic, softmax_step(): totals = totals * fading + jnp.sum(weights, axis=-1)  14 us
    dot_general x8, matrix products, softmax_step(): jnp.einsum(form, weights.astype(jnp.bfloat16), seg_values, preferred_elem...  10.9 us
    all_to_all x1, blocking collectives, body(): lax.all_to_all(sent_keys, 'tp', split_axis=1, concat_axis=0, tiled=True)  10.6 us
    all_gather x1, blocking collectives, body(): segment = lax.all_gather(target_normed, 'tp', axis=0, tiled=True)  9.97 us
    all_to_all x1, blocking collectives, body(): lax.all_to_all(sent_values, 'tp', split_axis=1, concat_axis=0, tiled=True)  8.6 us
  transfers between devices with their start and end apart: 3, of which 3 were waited for; matrix products, arithmetic and copies ran while one was open for 3% of the time, Pallas kernels for 0%

commit v1 on v0

--- a/solution.py
+++ b/solution.py
@@ -1,8 +1,11 @@
+import functools
 import math
 
 import jax
 import jax.numpy as jnp
 from jax import lax
+from jax.experimental import pallas as pl
+from jax.experimental.pallas import tpu as pltpu
 from jax.sharding import PartitionSpec as P
 
 KEY_VALUE_HEADS = 2
@@ -133,9 +136,418 @@
     return (target.astype(jnp.float32) + update).astype(jnp.bfloat16)
 
 
+MESH = pl.DeviceIdType.MESH
+CORES = 2
+
+
+def fused_kernel(
+    n_sp,
+    n_tp,
+    target_hbm,
+    source_hbm,
+    target_gain,
+    source_gain,
+    query_hbm,
+    key_hbm,
+    value_hbm,
+    query_gain,
+    key_gain,
+    out_hbm,
+    update,
+    target_in,
+    source_in,
+    query_w,
+    key_w,
+    value_w,
+    out_w,
+    targets,
+    queries,
+    pairs,
+    foreign,
+    maxima,
+    totals,
+    weighted,
+    outgoing,
+    incoming,
+    load_sem,
+    target_send,
+    target_recv,
+    z_send,
+    z_recv,
+    y_send,
+    y_recv,
+    x_send,
+    x_recv,
+    d_send,
+    d_recv,
+    out_send,
+    out_recv,
+):
+    planes = n_sp // CORES
+    sp = lax.axis_index("sp")
+    tp = lax.axis_index("tp")
+    z, core = sp // CORES, sp % CORES
+    y, x = tp // 2, tp % 2
+    tp_x = y * 2 + (1 - x)
+    tp_y = (1 - y) * 2 + x
+    tp_xy = (1 - y) * 2 + (1 - x)
+    mate = z * CORES + (1 - core)
+    above, below = sp + CORES, sp - CORES
+    head = HEAD_SIZE
+    rows_t = target_in.shape[0]
+    rows_s = source_in.shape[0]
+    heads = query_gain.shape[0]
+    rows_q = n_tp * rows_t
+
+    loads = [
+        pltpu.make_async_copy(a, b, load_sem.at[n])
+        for n, (a, b) in enumerate(
+            (
+                (target_hbm, target_in),
+                (source_hbm, source_in),
+                (key_hbm, key_w),
+                (value_hbm, value_w),
+                (query_hbm, query_w),
+                (out_hbm, out_w),
+            )
+        )
+    ]
+    for load in loads:
+        load.start()
+
+    barrier = pltpu.get_barrier_semaphore()
+    for peer in ((sp, tp_x), (sp, tp_y), (sp, tp_xy), (mate, tp)):
+        pl.semaphore_signal(barrier, inc=1, device_id=peer, device_id_type=MESH)
+
+    @pl.when(z > 0)
+    def _():
+        pl.semaphore_signal(barrier, inc=1, device_id=(below, tp), device_id_type=MESH)
+
+    @pl.when(z < planes - 1)
+    def _():
+        pl.semaphore_signal(barrier, inc=1, device_id=(above, tp), device_id_type=MESH)
+
+    def remote(src, dst, send, recv, peer):
+        return pltpu.make_async_remote_copy(
+            src_ref=src,
+            dst_ref=dst,
+            send_sem=send,
+            recv_sem=recv,
+            device_id=peer,
+            device_id_type=MESH,
+        )
+
+    loads[0].wait()
+    targets[tp] = normed(target_in[...].astype(jnp.float32), target_gain[...]).astype(jnp.bfloat16)
+
+    pl.semaphore_wait(barrier, 4 + jnp.minimum(z, 1) + jnp.minimum(planes - 1 - z, 1))
+
+    def target_copy(slot, n, peer):
+        return remote(
+            targets.at[slot], targets.at[slot], target_send.at[n], target_recv.at[n], peer
+        )
+
+    target_x = target_copy(tp, 0, (sp, tp_x))
+    target_y = target_copy(tp, 1, (sp, tp_y))
+    target_relay = target_copy(tp_x, 2, (sp, tp_y))
+    target_x.start()
+    target_y.start()
+
+    loads[1].wait()
+    source_normed = normed(source_in[...].astype(jnp.float32), source_gain[...]).astype(
+        jnp.bfloat16
+    )
+    loads[2].wait()
+    raw_keys = jnp.dot(source_normed, key_w[...], preferred_element_type=jnp.float32)
+    loads[3].wait()
+    raw_values = jnp.dot(source_normed, value_w[...], preferred_element_type=jnp.float32)
+
+    made = []
+    for h in range(KEY_VALUE_HEADS):
+        cut = slice(h * head, (h + 1) * head)
+        keys = normed(raw_keys[:, cut], key_gain[h : h + 1, :]).astype(jnp.bfloat16)
+        made.append((keys, raw_values[:, cut].astype(jnp.bfloat16)))
+    mine_zero = y == 0
+    for part in range(2):
+        cut = slice(part * head, (part + 1) * head)
+        pairs[z, tp, core, :, cut] = jnp.where(mine_zero, made[0][part], made[1][part])
+        foreign[z, :, cut] = jnp.where(mine_zero, made[1][part], made[0][part])
+
+    def z_copies(at, up):
+        peer = (above if up else below, tp)
+        own = pairs.at[at, tp, core]
+        other = foreign.at[at]
+        way = 0 if up else 1
+        return (
+            remote(own, own, z_send.at[0, way, at], z_recv.at[0, at], peer),
+            remote(other, other, z_send.at[1, way, at], z_recv.at[1, at], peer),
+        )
+
+    def along_z(at, act):
+        @pl.when(jnp.logical_and(at <= z, z < planes - 1))
+        def _():
+            for copy in z_copies(at, True):
+                act(copy)
+
+        @pl.when(jnp.logical_and(at >= z, z > 0))
+        def _():
+            for copy in z_copies(at, False):
+                act(copy)
+
+    def y_copy(at):
+        return remote(
+            foreign.at[at], pairs.at[at, tp, core], y_send.at[at], y_recv.at[at], (sp, tp_y)
+        )
+
+    def y_arrival(at):
+        return remote(
+            foreign.at[at], pairs.at[at, tp_y, core], y_send.at[at], y_recv.at[at], (sp, tp_y)
+        )
+
+    def x_copy(at, n, slot):
+        block = pairs.at[at, slot, core]
+        return remote(block, block, x_send.at[n, at], x_recv.at[n, at], (sp, tp_x))
+
+    slots = (tp, tp_y, tp_x, tp_xy)
+
+    def d_copy(at, n):
+        block = pairs.at[at, slots[n], core]
+        return remote(block, block, d_send.at[n, at], d_recv.at[n, at], (mate, tp))
+
+    def d_arrival(at, n):
+        block = pairs.at[at, slots[n], 1 - core]
+        return remote(block, block, d_send.at[n, at], d_recv.at[n, at], (mate, tp))
+
+    def place(turn):
+        other = planes - 1 - z
+        near = jnp.minimum(z, other)
+        step = (turn + 1) // 2
+        signed = z + step * (1 - 2 * (turn % 2))
+        far = jnp.where(z < other, turn, planes - 1 - turn)
+        return jnp.where(turn <= 2 * near, signed, far)
+
+    def launch(at):
+        along_z(at, lambda copy: copy.start())
+        x_copy(at, 0, tp).start()
+        y_copy(at).start()
+        d_copy(at, 0).start()
+
+    def relay_y(at):
+        y_arrival(at).wait_recv()
+        x_copy(at, 1, tp_y).start()
+        d_copy(at, 1).start()
+
+    def take_x(at):
+        x_copy(at, 0, tp_x).wait_recv()
+        d_copy(at, 2).start()
+        x_copy(at, 1, tp_xy).wait_recv()
+        d_copy(at, 3).start()
+
+    scale = math.log2(math.e) / math.sqrt(head)
+
+    def attend(at, n):
+        d_arrival(at, n).wait_recv()
+        both = pairs[at, slots[n]].reshape(CORES * rows_s, 2 * head)
+        scores = lax.dot_general(
+            both[:, :head],
+            queries[...],
+            (((1,), (1,)), ((), ())),
+            preferred_element_type=jnp.float32,
+        )
+        before = maxima[...]
+        after = jnp.maximum(before, jnp.max(scores, axis=0, keepdims=True))
+        weights = jnp.exp2((scores - after) * scale)
+        fading = jnp.exp2((before - after) * scale)
+        maxima[...] = after
+        totals[...] = totals[...] * fading + jnp.sum(weights, axis=0, keepdims=True)
+        weighted[...] = weighted[...] * fading + lax.dot_general(
+            both[:, head:],
+            weights.astype(jnp.bfloat16),
+            (((0,), (0,)), ((), ())),
+            preferred_element_type=jnp.float32,
+        )
+
+    launch(z)
+
+    maxima[...] = jnp.full(maxima.shape, -1e30, jnp.float32)
+    totals[...] = jnp.zeros(totals.shape, jnp.float32)
+    weighted[...] = jnp.zeros(weighted.shape, jnp.float32)
+
+    target_copy(tp_x, 0, (sp, tp_x)).wait_recv()
+    target_relay.start()
+    target_copy(tp_y, 1, (sp, tp_y)).wait_recv()
+    relay_y(z)
+    target_copy(tp_xy, 2, (sp, tp_y)).wait_recv()
+    loads[4].wait()
+    all_targets = targets[...].reshape(rows_q, targets.shape[2])
+    raw = jnp.dot(all_targets, query_w[...], preferred_element_type=jnp.float32)
+    for h in range(heads):
+        queries[h * rows_q : (h + 1) * rows_q, :] = normed(
+            raw[:, h * head : (h + 1) * head], query_gain[h : h + 1, :]
+        ).astype(jnp.bfloat16)
+
+    def one_turn(turn, carried):
+        at = place(turn)
+        prior = place(turn - 1)
+        for part in range(2):
+            z_copies(at, True)[part].wait_recv()
+        launch(at)
+        take_x(prior)
+        attend(prior, 0)
+        attend(prior, 1)
+        relay_y(at)
+        attend(prior, 2)
+        attend(prior, 3)
+        return carried
+
+    lax.fori_loop(1, planes, one_turn, 0)
+    last = place(planes - 1)
+    attend(last, 0)
+    attend(last, 1)
+    take_x(last)
+    attend(last, 2)
+    attend(last, 3)
+
+    shared = weighted[...] / totals[...]
+    attended = jnp.concatenate(
+        [shared[:, h * rows_q : (h + 1) * rows_q].T for h in range(heads)], axis=1
+    ).astype(jnp.bfloat16)
+    loads[5].wait()
+    held = queries
+    for h in range(heads):
+        held[h * rows_q : (h + 1) * rows_q, :] = attended[:, h * head : (h + 1) * head]
+
+    def product(slot):
+        rows = jnp.concatenate(
+            [
+                held[pl.ds(pl.multiple_of(h * rows_q + slot * rows_t, rows_t), rows_t), :]
+                for h in range(heads)
+            ],
+            axis=1,
+        )
+        return jnp.dot(rows, out_w[...], preferred_element_type=jnp.float32)
+
+    sends = []
+    for n, peer in enumerate((tp_xy, tp_x, tp_y)):
+        outgoing[n] = product(peer).astype(jnp.bfloat16)
+        copy = remote(outgoing.at[n], incoming.at[n], out_send.at[n], out_recv.at[n], (sp, peer))
+        copy.start()
+        sends.append(copy)
+    mine = product(tp)
+    for copy in (target_x, target_y, target_relay):
+        copy.wait_send()
+
+    def drain(at, carried):
+        along_z(at, lambda copy: copy.wait_send())
+        y_copy(at).wait_send()
+        x_copy(at, 0, tp).wait_send()
+        x_copy(at, 1, tp_y).wait_send()
+        for n in range(4):
+            d_copy(at, n).wait_send()
+        return carried
+
+    lax.fori_loop(0, planes, drain, 0)
+    for copy in sends:
+        copy.wait_recv()
+    update[...] = mine + (
+        incoming[0].astype(jnp.float32)
+        + incoming[1].astype(jnp.float32)
+        + incoming[2].astype(jnp.float32)
+    )
+    for copy in sends:
+        copy.wait_send()
+
+
+def fused_body(
+    n_sp,
+    n_tp,
+    target,
+    source,
+    target_gain,
+    source_gain,
+    query_weight,
+    key_matrix,
+    value_matrix,
+    query_gain,
+    key_gain,
+    out_weight,
+):
+    rows_t, width = target.shape
+    rows_s = source.shape[0]
+    planes = n_sp // CORES
+    heads = query_gain.shape[0]
+    lanes = heads * n_tp * rows_t
+    bf16, f32 = jnp.bfloat16, jnp.float32
+    dma = pltpu.SemaphoreType.DMA
+    any_spec = pl.BlockSpec(memory_space=pl.ANY)
+    vmem_spec = pl.BlockSpec(memory_space=pltpu.VMEM)
+    update = pl.pallas_call(
+        functools.partial(fused_kernel, n_sp, n_tp),
+        out_shape=jax.ShapeDtypeStruct((rows_t, width), f32),
+        in_specs=[
+            any_spec,
+            any_spec,
+            vmem_spec,
+            vmem_spec,
+            any_spec,
+            any_spec,
+            any_spec,
+            vmem_spec,
+            vmem_spec,
+            any_spec,
+        ],
+        out_specs=vmem_spec,
+        scratch_shapes=[
+            pltpu.VMEM(target.shape, bf16),
+            pltpu.VMEM(source.shape, bf16),
+            pltpu.VMEM(query_weight.shape, bf16),
+            pltpu.VMEM(key_matrix.shape, bf16),
+            pltpu.VMEM(value_matrix.shape, bf16),
+            pltpu.VMEM(out_weight.shape, bf16),
+            pltpu.VMEM((n_tp, rows_t, width), bf16),
+            pltpu.VMEM((lanes, HEAD_SIZE), bf16),
+            pltpu.VMEM((planes, n_tp, CORES, rows_s, 2 * HEAD_SIZE), bf16),
+            pltpu.VMEM((planes, rows_s, 2 * HEAD_SIZE), bf16),
+            pltpu.VMEM((1, lanes), f32),
+            pltpu.VMEM((1, lanes), f32),
+            pltpu.VMEM((HEAD_SIZE, lanes), f32),
+            pltpu.VMEM((3, rows_t, width), bf16),
+            pltpu.VMEM((3, rows_t, width), bf16),
+            dma((6,)),
+            dma((3,)),
+            dma((3,)),
+            dma((2, 2, planes)),
+            dma((2, planes)),
+            dma((planes,)),
+            dma((planes,)),
+            dma((2, planes)),
+            dma((2, planes)),
+            dma((4, planes)),
+            dma((4, planes)),
+            dma((3,)),
+            dma((3,)),
+        ],
+        compiler_params=pltpu.CompilerParams(collective_id=0, has_side_effects=True),
+    )(
+        target,
+        source,
+        target_gain.reshape(1, -1),
+        source_gain.reshape(1, -1),
+        query_weight,
+        key_matrix,
+        value_matrix,
+        query_gain,
+        key_gain,
+        out_weight,
+    )
+    return (target.astype(f32) + update).astype(bf16)
+
+
 def solution(mesh):
+    sp, tp = mesh.shape["sp"], mesh.shape["tp"]
+    fits = tp == 2 * KEY_VALUE_HEADS and sp % 2 == 0
     return jax.shard_map(
-        body,
+        functools.partial(fused_body, sp, tp) if fits else body,
         mesh=mesh,
         in_specs=(
             P(("sp", "tp"), None),

time: 153 us -> 51.9 us (0.34)
  waiting for transfers between devices: 52.1 us -> 0 us
  Pallas kernels: 0 us -> 50.1 us
  matrix products: 37.3 us -> 0 us
  blocking collectives: 29.2 us -> 0 us
  other arithmetic: 18.5 us -> 1.63 us
  between operations: 13.4 us -> 0.02 us
    pallas_call x0 -> x1, Pallas kernels: none -> 50.1 us  [fused_body(): pl.pallas_call(functools.partial(fused_kernel, n_sp, n_tp), out_shape=jax...]
    dot_general x20 -> x0, matrix products: 37.3 us -> none  [the longest x8 19.4 us: advance(): jnp.einsum('rhd,nd->rhn', query_vectors, portion[0], preferred_element_ty...]
    all_gather x2 -> x0, waiting for transfers between devices: 27.7 us -> none  [the longest x1 26.1 us: body(): lax.all_gather(head_values, 'sp', axis=0, tiled=True)]
    reduce_scatter x1 -> x0, waiting for transfers between devices: 24.4 us -> none  [body(): lax.psum_scatter(jnp.dot(portion, out_weight, preferred_element_type=jnp....]
    all_to_all x2 -> x0, blocking collectives: 19.2 us -> none  [the longest x1 10.6 us: body(): lax.all_to_all(sent_keys, 'tp', split_axis=1, concat_axis=0, tiled=True)]
    reduce_sum x12 -> x0, other arithmetic: 16.1 us -> none  [the longest x8 14 us: softmax_step(): totals = totals * fading + jnp.sum(weights, axis=-1)]
    all_gather x1 -> x0, blocking collectives: 9.97 us -> none  [body(): segment = lax.all_gather(target_normed, 'tp', axis=0, tiled=True)]
  transfers between devices with their start and end apart: 3 -> 0, of which waited for: 3 -> 0; matrix products, arithmetic and copies ran while one was open for 3% -> 0% of each run, Pallas kernels for 0% -> 0%
where the time goes in v1:
time: 51.9 us; the launch traced here: 51.7 us
  Pallas kernels  50.1 us (97%)
  other arithmetic  1.63 us (3%)
    pallas_call x1, Pallas kernels, fused_body(): pl.pallas_call(functools.partial(fused_kernel, n_sp, n_tp), out_shape=jax...  50.1 us
    convert_element_type x1, other arithmetic, fused_body(): return (target.astype(f32) + update).astype(bf16)  1.63 us

profile of v1, /device:TPU:0, one launch (start us, length us, event | category | flops | bytes accessed | tf_op | source)
XLA Modules:
  0.0 51.7 jit_solution(8155730379861849120)
XLA Ops:
  0.0 0.0 copy-start
  0.0 50.1 %shard_map.100 = f32[32,2048]{1,0:T(8,128)} custom-call(bf16[32,2048]{1,0:T(8,128)(2,1)} %target_hbm.1, bf16[192,2048]{1,0:T(8,128)(2,1)} %source_hbm.1, f32[1,2048]{1,0:T(1,128)} %bitcast.2, f32[1,2048]{1,0:T(1,128)} %bitcast.3, bf16[2048,512]{1,0:T(8,128)(2,1)} %query_hbm.1, bf16[2048,256]{1,0:T(8,128)(2,1)} %key_hbm.1, bf16[2048,256]{1,0:T(8,128)(2,1)} %value_hbm.1, ...), custom_call_target="tpu_custom_call" | custom-call | tf_op jit(solution)/shard_map/pallas_call | solution.py:484
  50.1 0.0 copy-done
  50.1 1.6 %add_convert_fusion = bf16[32,2048]{1,0:T(8,128)(2,1)} fusion(f32[32,2048]{1,0:T(8,128)} %shard_map.100, bf16[32,2048]{1,0:T(8,128)(2,1)S(1)} %copy-done), kind=kLoop, calls=%fused_computation | loop fusion | flops 196608 | bytes 524288 | tf_op jit(solution)/shard_map/convert_element_type | solution.py:543
Async XLA Ops:
  0.0 50.1 %copy-start = (bf16[32,2048]{1,0:T(8,128)(2,1)S(1)}, bf16[32,2048]{1,0:T(8,128)(2,1)}, u32[]{:S(2)}) copy-start(bf16[32,2048]{1,0:T(8,128)(2,1)} %target_hbm.1) | copy-start | bytes 393220

commit v2 on v1

--- a/solution.py
+++ b/solution.py
@@ -167,6 +167,11 @@
     maxima,
     totals,
     weighted,
+    held,
+    part_out,
+    part_in,
+    stats_out,
+    stats_in,
     outgoing,
     incoming,
     load_sem,
@@ -271,44 +276,33 @@
     for part in range(2):
         cut = slice(part * head, (part + 1) * head)
         pairs[z, tp, core, :, cut] = jnp.where(mine_zero, made[0][part], made[1][part])
-        foreign[z, :, cut] = jnp.where(mine_zero, made[1][part], made[0][part])
-
-    def z_copies(at, up):
+        foreign[:, cut] = jnp.where(mine_zero, made[1][part], made[0][part])
+
+    def z_copy(at, n, up):
+        block = pairs.at[at, slots[n], core]
+        way = 0 if up else 1
         peer = (above if up else below, tp)
-        own = pairs.at[at, tp, core]
-        other = foreign.at[at]
-        way = 0 if up else 1
-        return (
-            remote(own, own, z_send.at[0, way, at], z_recv.at[0, at], peer),
-            remote(other, other, z_send.at[1, way, at], z_recv.at[1, at], peer),
-        )
-
-    def along_z(at, act):
+        return remote(block, block, z_send.at[n, way, at], z_recv.at[n, at], peer)
+
+    def along_z(at, n, act):
         @pl.when(jnp.logical_and(at <= z, z < planes - 1))
         def _():
-            for copy in z_copies(at, True):
-                act(copy)
+            act(z_copy(at, n, True))
 
         @pl.when(jnp.logical_and(at >= z, z > 0))
         def _():
-            for copy in z_copies(at, False):
-                act(copy)
-
-    def y_copy(at):
-        return remote(
-            foreign.at[at], pairs.at[at, tp, core], y_send.at[at], y_recv.at[at], (sp, tp_y)
-        )
-
-    def y_arrival(at):
-        return remote(
-            foreign.at[at], pairs.at[at, tp_y, core], y_send.at[at], y_recv.at[at], (sp, tp_y)
-        )
-
-    def x_copy(at, n, slot):
-        block = pairs.at[at, slot, core]
-        return remote(block, block, x_send.at[n, at], x_recv.at[n, at], (sp, tp_x))
-
-    slots = (tp, tp_y, tp_x, tp_xy)
+            act(z_copy(at, n, False))
+
+    def y_copy(slot):
+        return remote(foreign, pairs.at[z, slot, core], y_send.at[0], y_recv.at[0], (sp, tp_y))
+
+    def x_copy(src, dst, n):
+        return remote(src, dst, x_send.at[n], x_recv.at[n], (sp, tp_x))
+
+    query_copy = x_copy(queries.at[0], queries.at[1], 0)
+    part_copy = x_copy(part_out, part_in, 1)
+    stats_copy = x_copy(stats_out, stats_in, 2)
+    slots = (tp, tp_y)
 
     def d_copy(at, n):
         block = pairs.at[at, slots[n], core]
@@ -326,48 +320,42 @@
         far = jnp.where(z < other, turn, planes - 1 - turn)
         return jnp.where(turn <= 2 * near, signed, far)
 
-    def launch(at):
-        along_z(at, lambda copy: copy.start())
-        x_copy(at, 0, tp).start()
-        y_copy(at).start()
-        d_copy(at, 0).start()
-
-    def relay_y(at):
-        y_arrival(at).wait_recv()
-        x_copy(at, 1, tp_y).start()
-        d_copy(at, 1).start()
-
-    def take_x(at):
-        x_copy(at, 0, tp_x).wait_recv()
-        d_copy(at, 2).start()
-        x_copy(at, 1, tp_xy).wait_recv()
-        d_copy(at, 3).start()
+    def launch(at, n):
+        along_z(at, n, lambda copy: copy.start())
+        d_copy(at, n).start()
+
+    def take_z(at, n):
+        z_copy(at, n, True).wait_recv()
+        launch(at, n)
 
     scale = math.log2(math.e) / math.sqrt(head)
 
-    def attend(at, n):
+    def ready(at, n):
         d_arrival(at, n).wait_recv()
+
+    def attend(at, n, half):
         both = pairs[at, slots[n]].reshape(CORES * rows_s, 2 * head)
         scores = lax.dot_general(
             both[:, :head],
-            queries[...],
+            queries[half],
             (((1,), (1,)), ((), ())),
             preferred_element_type=jnp.float32,
         )
-        before = maxima[...]
+        before = maxima[half]
         after = jnp.maximum(before, jnp.max(scores, axis=0, keepdims=True))
         weights = jnp.exp2((scores - after) * scale)
         fading = jnp.exp2((before - after) * scale)
-        maxima[...] = after
-        totals[...] = totals[...] * fading + jnp.sum(weights, axis=0, keepdims=True)
-        weighted[...] = weighted[...] * fading + lax.dot_general(
+        maxima[half] = after
+        totals[half] = totals[half] * fading + jnp.sum(weights, axis=0, keepdims=True)
+        weighted[half] = weighted[half] * fading + lax.dot_general(
             both[:, head:],
             weights.astype(jnp.bfloat16),
             (((0,), (0,)), ((), ())),
             preferred_element_type=jnp.float32,
         )
 
-    launch(z)
+    y_copy(tp).start()
+    launch(z, 0)
 
     maxima[...] = jnp.full(maxima.shape, -1e30, jnp.float32)
     totals[...] = jnp.zeros(totals.shape, jnp.float32)
@@ -376,44 +364,61 @@
     target_copy(tp_x, 0, (sp, tp_x)).wait_recv()
     target_relay.start()
     target_copy(tp_y, 1, (sp, tp_y)).wait_recv()
-    relay_y(z)
+    y_copy(tp_y).wait_recv()
+    launch(z, 1)
     target_copy(tp_xy, 2, (sp, tp_y)).wait_recv()
     loads[4].wait()
     all_targets = targets[...].reshape(rows_q, targets.shape[2])
     raw = jnp.dot(all_targets, query_w[...], preferred_element_type=jnp.float32)
     for h in range(heads):
-        queries[h * rows_q : (h + 1) * rows_q, :] = normed(
+        queries[0, h * rows_q : (h + 1) * rows_q, :] = normed(
             raw[:, h * head : (h + 1) * head], query_gain[h : h + 1, :]
         ).astype(jnp.bfloat16)
+
+    query_copy.start()
 
     def one_turn(turn, carried):
         at = place(turn)
         prior = place(turn - 1)
-        for part in range(2):
-            z_copies(at, True)[part].wait_recv()
-        launch(at)
-        take_x(prior)
-        attend(prior, 0)
-        attend(prior, 1)
-        relay_y(at)
-        attend(prior, 2)
-        attend(prior, 3)
+        take_z(at, 0)
+        ready(prior, 0)
+        attend(prior, 0, 0)
+        take_z(at, 1)
+        ready(prior, 1)
+        attend(prior, 1, 0)
+
+        @pl.when(turn == 1)
+        def _():
+            query_copy.wait_recv()
+
+        attend(prior, 0, 1)
+        attend(prior, 1, 1)
         return carried
 
     lax.fori_loop(1, planes, one_turn, 0)
     last = place(planes - 1)
-    attend(last, 0)
-    attend(last, 1)
-    take_x(last)
-    attend(last, 2)
-    attend(last, 3)
-
-    shared = weighted[...] / totals[...]
+    ready(last, 0)
+    attend(last, 0, 1)
+    ready(last, 1)
+    attend(last, 1, 1)
+    part_out[...] = (weighted[1] / totals[1]).astype(jnp.bfloat16)
+    stats_out[0:1, :] = maxima[1]
+    stats_out[1:2, :] = totals[1]
+    part_copy.start()
+    stats_copy.start()
+    attend(last, 0, 0)
+    attend(last, 1, 0)
+    loads[5].wait()
+    stats_copy.wait_recv()
+    highest = jnp.maximum(maxima[0], stats_in[0:1, :])
+    fading_own = jnp.exp2((maxima[0] - highest) * scale)
+    counted = stats_in[1:2, :] * jnp.exp2((stats_in[0:1, :] - highest) * scale)
+    everything = totals[0] * fading_own + counted
+    part_copy.wait_recv()
+    shared = (weighted[0] * fading_own + part_in[...].astype(jnp.float32) * counted) / everything
     attended = jnp.concatenate(
         [shared[:, h * rows_q : (h + 1) * rows_q].T for h in range(heads)], axis=1
     ).astype(jnp.bfloat16)
-    loads[5].wait()
-    held = queries
     for h in range(heads):
         held[h * rows_q : (h + 1) * rows_q, :] = attended[:, h * head : (h + 1) * head]
 
@@ -434,15 +439,14 @@
         copy.start()
         sends.append(copy)
     mine = product(tp)
-    for copy in (target_x, target_y, target_relay):
+    for copy in (target_x, target_y, target_relay, query_copy, part_copy, stats_copy):
         copy.wait_send()
 
+    y_copy(tp).wait_send()
+
     def drain(at, carried):
-        along_z(at, lambda copy: copy.wait_send())
-        y_copy(at).wait_send()
-        x_copy(at, 0, tp).wait_send()
-        x_copy(at, 1, tp_y).wait_send()
-        for n in range(4):
+        for n in range(2):
+            along_z(at, n, lambda copy: copy.wait_send())
             d_copy(at, n).wait_send()
         return carried
 
@@ -505,12 +509,17 @@
             pltpu.VMEM(value_matrix.shape, bf16),
             pltpu.VMEM(out_weight.shape, bf16),
             pltpu.VMEM((n_tp, rows_t, width), bf16),
+            pltpu.VMEM((2, lanes, HEAD_SIZE), bf16),
+            pltpu.VMEM((planes, n_tp, CORES, rows_s, 2 * HEAD_SIZE), bf16),
+            pltpu.VMEM((rows_s, 2 * HEAD_SIZE), bf16),
+            pltpu.VMEM((2, 1, lanes), f32),
+            pltpu.VMEM((2, 1, lanes), f32),
+            pltpu.VMEM((2, HEAD_SIZE, lanes), f32),
             pltpu.VMEM((lanes, HEAD_SIZE), bf16),
-            pltpu.VMEM((planes, n_tp, CORES, rows_s, 2 * HEAD_SIZE), bf16),
-            pltpu.VMEM((planes, rows_s, 2 * HEAD_SIZE), bf16),
-            pltpu.VMEM((1, lanes), f32),
-            pltpu.VMEM((1, lanes), f32),
-            pltpu.VMEM((HEAD_SIZE, lanes), f32),
+            pltpu.VMEM((HEAD_SIZE, lanes), bf16),
+            pltpu.VMEM((HEAD_SIZE, lanes), bf16),
+            pltpu.VMEM((2, lanes), f32),
+            pltpu.VMEM((2, lanes), f32),
             pltpu.VMEM((3, rows_t, width), bf16),
             pltpu.VMEM((3, rows_t, width), bf16),
             dma((6,)),
@@ -518,12 +527,12 @@
             dma((3,)),
             dma((2, 2, planes)),
             dma((2, planes)),
-            dma((planes,)),
-            dma((planes,)),
+            dma((1,)),
+            dma((1,)),
+            dma((3,)),
+            dma((3,)),
             dma((2, planes)),
             dma((2, planes)),
-            dma((4, planes)),
-            dma((4, planes)),
             dma((3,)),
             dma((3,)),
         ],
@@ -545,7 +554,7 @@
 
 def solution(mesh):
     sp, tp = mesh.shape["sp"], mesh.shape["tp"]
-    fits = tp == 2 * KEY_VALUE_HEADS and sp % 2 == 0
+    fits = tp == 2 * KEY_VALUE_HEADS and sp % CORES == 0 and sp > CORES
     return jax.shard_map(
         functools.partial(fused_body, sp, tp) if fits else body,
         mesh=mesh,

time: 51.9 us -> 45.7 us (0.88)
  Pallas kernels: 50.1 us -> 43.9 us
    pallas_call x1, Pallas kernels: 50.1 us -> 43.9 us  [fused_body(): pl.pallas_call(functools.partial(fused_kernel, n_sp, n_tp), out_shape=jax...]
where the time goes in v2:
time: 45.7 us; the launch traced here: 45.5 us
  Pallas kernels  43.9 us (96%)
  other arithmetic  1.63 us (4%)
    pallas_call x1, Pallas kernels, fused_body(): pl.pallas_call(functools.partial(fused_kernel, n_sp, n_tp), out_shape=jax...  43.9 us
    convert_element_type x1, other arithmetic, fused_body(): return (target.astype(f32) + update).astype(bf16)  1.63 us

profile of v2, /device:TPU:0, one launch (start us, length us, event | category | flops | bytes accessed | tf_op | source)
XLA Modules:
  0.0 45.5 jit_solution(8191512279228318966)
XLA Ops:
  0.0 0.0 copy-start
  0.0 43.9 %shard_map.100 = f32[32,2048]{1,0:T(8,128)} custom-call(bf16[32,2048]{1,0:T(8,128)(2,1)} %target_hbm.1, bf16[192,2048]{1,0:T(8,128)(2,1)} %source_hbm.1, f32[1,2048]{1,0:T(1,128)} %bitcast.2, f32[1,2048]{1,0:T(1,128)} %bitcast.3, bf16[2048,512]{1,0:T(8,128)(2,1)} %query_hbm.1, bf16[2048,256]{1,0:T(8,128)(2,1)} %key_hbm.1, bf16[2048,256]{1,0:T(8,128)(2,1)} %value_hbm.1, ...), custom_call_target="tpu_custom_call" | custom-call | tf_op jit(solution)/shard_map/pallas_call | solution.py:488
  43.9 0.0 copy-done
  43.9 1.6 %add_convert_fusion = bf16[32,2048]{1,0:T(8,128)(2,1)} fusion(f32[32,2048]{1,0:T(8,128)} %shard_map.100, bf16[32,2048]{1,0:T(8,128)(2,1)S(1)} %copy-done), kind=kLoop, calls=%fused_computation | loop fusion | flops 196608 | bytes 524288 | tf_op jit(solution)/shard_map/convert_element_type | solution.py:552
Async XLA Ops:
  0.0 43.9 %copy-start = (bf16[32,2048]{1,0:T(8,128)(2,1)S(1)}, bf16[32,2048]{1,0:T(8,128)(2,1)}, u32[]{:S(2)}) copy-start(bf16[32,2048]{1,0:T(8,128)(2,1)} %target_hbm.1) | copy-start | bytes 393220

commit v3 on v2

--- a/solution.py
+++ b/solution.py
@@ -387,12 +387,17 @@
         ready(prior, 1)
         attend(prior, 1, 0)
 
-        @pl.when(turn == 1)
+        @pl.when(turn == 2)
         def _():
             query_copy.wait_recv()
-
-        attend(prior, 0, 1)
-        attend(prior, 1, 1)
+            attend(z, 0, 1)
+            attend(z, 1, 1)
+
+        @pl.when(turn >= 2)
+        def _():
+            attend(prior, 0, 1)
+            attend(prior, 1, 1)
+
         return carried
 
     lax.fori_loop(1, planes, one_turn, 0)
@@ -554,7 +559,7 @@
 
 def solution(mesh):
     sp, tp = mesh.shape["sp"], mesh.shape["tp"]
-    fits = tp == 2 * KEY_VALUE_HEADS and sp % CORES == 0 and sp > CORES
+    fits = tp == 2 * KEY_VALUE_HEADS and sp % CORES == 0 and sp > 2 * CORES
     return jax.shard_map(
         functools.partial(fused_body, sp, tp) if fits else body,
         mesh=mesh,

time: 45.7 us -> 43.2 us (0.945)
  Pallas kernels: 43.9 us -> 41.4 us
    pallas_call x1, Pallas kernels: 43.9 us -> 41.4 us  [fused_body(): pl.pallas_call(functools.partial(fused_kernel, n_sp, n_tp), out_shape=jax...]
where the time goes in v3:
time: 43.2 us; the launch traced here: 43.1 us
  Pallas kernels  41.4 us (96%)
  other arithmetic  1.63 us (4%)
    pallas_call x1, Pallas kernels, fused_body(): pl.pallas_call(functools.partial(fused_kernel, n_sp, n_tp), out_shape=jax...  41.4 us
    convert_element_type x1, other arithmetic, fused_body(): return (target.astype(f32) + update).astype(bf16)  1.63 us

profile of v3, /device:TPU:0, one launch (start us, length us, event | category | flops | bytes accessed | tf_op | source)
XLA Modules:
  0.0 43.1 jit_solution(17877449612957519302)
XLA Ops:
  0.0 0.0 copy-start
  0.0 41.4 %shard_map.100 = f32[32,2048]{1,0:T(8,128)} custom-call(bf16[32,2048]{1,0:T(8,128)(2,1)} %target_hbm.1, bf16[192,2048]{1,0:T(8,128)(2,1)} %source_hbm.1, f32[1,2048]{1,0:T(1,128)} %bitcast.2, f32[1,2048]{1,0:T(1,128)} %bitcast.3, bf16[2048,512]{1,0:T(8,128)(2,1)} %query_hbm.1, bf16[2048,256]{1,0:T(8,128)(2,1)} %key_hbm.1, bf16[2048,256]{1,0:T(8,128)(2,1)} %value_hbm.1, ...), custom_call_target="tpu_custom_call" | custom-call | tf_op jit(solution)/shard_map/pallas_call | solution.py:493
  41.4 0.0 copy-done
  41.5 1.6 %add_convert_fusion = bf16[32,2048]{1,0:T(8,128)(2,1)} fusion(f32[32,2048]{1,0:T(8,128)} %shard_map.100, bf16[32,2048]{1,0:T(8,128)(2,1)S(1)} %copy-done), kind=kLoop, calls=%fused_computation | loop fusion | flops 196608 | bytes 524288 | tf_op jit(solution)/shard_map/convert_element_type | solution.py:557
Async XLA Ops:
  0.0 41.4 %copy-start = (bf16[32,2048]{1,0:T(8,128)(2,1)S(1)}, bf16[32,2048]{1,0:T(8,128)(2,1)}, u32[]{:S(2)}) copy-start(bf16[32,2048]{1,0:T(8,128)(2,1)} %target_hbm.1) | copy-start | bytes 393220
